TPU v7x, 32 devices: a whole 2x2x4 slice. The times are simulated.
32 devices in a mesh: sp: 16 (over z, y, x), tp: 2 (over core).
Axes of the slice: x: 2, y: 2, z: 4, core: 2. Of those that a mesh axis runs over, the one named last changes fastest.
Arguments:
- block_input: bfloat16 [1, 1024, 4096], P(None, 'sp', 'tp'), may hold values from -6 to 6
- key_weight: bfloat16 [4096, 2048], P('sp', 'tp'), may hold values from -0.09375 to 0.09375
- value_weight: bfloat16 [4096, 2048], P('sp', 'tp'), may hold values from -0.09375 to 0.09375
- earlier_keys: bfloat16 [1, 4096, 2048], P(None, 'sp', 'tp'), may hold values from -10 to 10
- past_values: bfloat16 [1, 4096, 2048], P(None, 'sp', 'tp'), may hold values from -6 to 6
- past_gates: float32 [1, 16, 4096], P(None, 'tp', 'sp'), may hold values from -770.15 to 0, as said below
- block_gates: float32 [1, 16, 1024], P(None, 'tp', 'sp'), may hold values from -770.15 to 0
- step_query: bfloat16 [1, 2048], P(None, 'tp'), may hold values from -12 to 12
- step_key: bfloat16 [1, 2048], P(None, 'tp'), may hold values from -10 to 10
- step_value: bfloat16 [1, 2048], P(None, 'tp'), may hold values from -6 to 6
- step_gate: float32 [1, 16], P(None, 'tp'), may hold values from -770.15 to 0, as said below
Outputs:
- cache_keys: bfloat16 [16, 320, 2048], P('sp', None, 'tp')
- stored_vector_entries: bfloat16 [16, 320, 2048], P('sp', None, 'tp')
- cache_gates: float32 [16, 16, 320], P('sp', 'tp')
- initial_attention_output: float32 [1, 2048], P(None, 'tp')
Inputs may be any that keep to these rules, and one draw needn't show every extreme that they name: Cumulative sums of negative log gates along each sequence and head; they never rise from one position to the next, and block_gates continue past_gates. `step_gate`: the cumulative log gate one position after the block, no larger than the block's last.
All inputs are finite; a program needn't handle non-finite values.
Results may differ from a plain program's by a relative error of at most 0.0055.
Values may be sent and summed in bfloat16 or wider, within the bound.
A program may use at most 64 MiB of HBM per device.

v0:
```python
import jax
import jax.numpy as jnp
from jax import lax
from jax.sharding import PartitionSpec as P

HEAD_DIM = 128
GROUP = 16


lowest_score_bound = -1e30


def merged_2(part, axis, combine):
    gathered = jax.tree.map(lambda a: lax.all_gather(a, axis), part)

    def take(source):
        return jax.tree.map(lambda a: lax.dynamic_index_in_dim(a, source, 0, False), gathered)

    return lax.fori_loop(
        1, lax.axis_size(axis), lambda source, state: combine(state, take(source)), take(0)
    )


def share_split(source_rows, shares):
    return source_rows.reshape(shares, -1, source_rows.shape[2])


def partial_read(queries, key_rows, value_rows, gate_rows, gate_here):
    sequences, row_count = (key_rows.shape[0], key_rows.shape[1])
    local_heads, head_width = (queries.shape[1], queries.shape[2])
    key_rows = key_rows.reshape(sequences, row_count, local_heads, head_width)
    value_rows = value_rows.reshape(sequences, row_count, local_heads, head_width)
    scores = jnp.einsum("shd,srhd->shr", queries, key_rows, preferred_element_type=jnp.float32)
    scores = scores * head_width ** (-0.5) + gate_here[:, :, None] - gate_rows
    maximum = jnp.max(scores, axis=2)
    weights = jnp.exp(scores - maximum[:, :, None])
    denominator = jnp.sum(weights, axis=2)
    summed = jnp.einsum(
        "shr,srhd->shd", weights, value_rows.astype(jnp.float32), precision=lax.Precision.HIGHEST
    )
    return (maximum, denominator, summed)


def combine_reads(former, latter):
    maximum = jnp.maximum(former[0], latter[0])
    former_scale = jnp.exp(former[0] - maximum)
    latter_scale = jnp.exp(latter[0] - maximum)
    return (
        maximum,
        former[1] * former_scale + latter[1] * latter_scale,
        former[2] * former_scale[:, :, None] + latter[2] * latter_scale[:, :, None],
    )


def local(
    block_input,
    key_weight,
    value_weight,
    earlier_keys,
    past_values,
    past_gates,
    block_gates,
    step_query,
    step_key,
    step_value,
    step_gate,
):
    sequences, span_rows = (block_input.shape[0], block_input.shape[1])
    local_width = key_weight.shape[1]
    local_heads = local_width // HEAD_DIM
    shares = sequences * GROUP
    past_parts = past_gates.reshape(sequences, local_heads, GROUP, -1)
    block_parts = block_gates.reshape(sequences, local_heads, GROUP, -1)
    gate_block_groups = (
        jnp.concatenate([past_parts, block_parts], axis=3)
        .transpose(0, 2, 1, 3)
        .reshape(shares, local_heads, -1)
    )
    cache_gates = lax.all_to_all(gate_block_groups, "sp", split_axis=0, concat_axis=2, tiled=True)
    gathered = lax.all_gather(block_input, "tp", axis=2, tiled=True)
    flat_input = gathered.reshape(sequences * span_rows, gathered.shape[2])
    key_sums = jnp.dot(
        flat_input,
        lax.all_gather(key_weight, "sp", axis=0, tiled=True),
        preferred_element_type=jnp.float32,
    )
    value_sums = jnp.dot(
        flat_input,
        lax.all_gather(value_weight, "sp", axis=0, tiled=True),
        preferred_element_type=jnp.float32,
    )
    block_keys = key_sums.astype(jnp.bfloat16).reshape(sequences, span_rows, local_width)
    block_values = value_sums.astype(jnp.bfloat16).reshape(sequences, span_rows, local_width)
    joined_keys = jnp.concatenate(
        [share_split(earlier_keys, shares), share_split(block_keys, shares)], axis=1
    )
    assembled_vector_entries = jnp.concatenate(
        [share_split(past_values, shares), share_split(block_values, shares)], axis=1
    )
    cache_keys, stored_vector_entries = (
        lax.all_to_all(joined_keys, "sp", split_axis=0, concat_axis=1, tiled=True),
        lax.all_to_all(assembled_vector_entries, "sp", split_axis=0, concat_axis=1, tiled=True),
    )
    queries = step_query.reshape(sequences, local_heads, HEAD_DIM)
    owner_seq = lax.axis_index("sp") // GROUP
    own_query = lax.dynamic_slice_in_dim(queries, owner_seq, 1, 0)
    own_gate = lax.dynamic_slice_in_dim(step_gate, owner_seq, 1, 0)
    maximum, denominator, summed = partial_read(
        own_query, cache_keys, stored_vector_entries, cache_gates, own_gate
    )
    chosen = (jnp.arange(sequences, dtype=jnp.int32) == owner_seq)[:, None]
    partial_value = (
        jnp.where(chosen, maximum, lowest_score_bound),
        jnp.where(chosen, denominator, 0.0),
        jnp.where(chosen[:, :, None], summed, 0.0),
    )
    merged = merged_2(partial_value, "sp", combine_reads)
    own_keys = step_key.reshape(sequences, local_heads, HEAD_DIM).astype(jnp.float32)
    own_values = step_value.reshape(sequences, local_heads, HEAD_DIM).astype(jnp.float32)
    own_score = jnp.sum(queries.astype(jnp.float32) * own_keys, axis=2) * HEAD_DIM ** (-0.5)
    maximum = jnp.maximum(merged[0], own_score)
    kept_scale = jnp.exp(merged[0] - maximum)
    fresh_weight = jnp.exp(own_score - maximum)
    denominator = merged[1] * kept_scale + fresh_weight
    summed = merged[2] * kept_scale[:, :, None] + fresh_weight[:, :, None] * own_values
    initial_attention_output = (summed / denominator[:, :, None]).reshape(sequences, local_width)
    return (cache_keys, stored_vector_entries, cache_gates, initial_attention_output)


def solution(mesh):
    in_specs = (
        P(None, "sp", "tp"),
        P("sp", "tp"),
        P("sp", "tp"),
        P(None, "sp", "tp"),
        P(None, "sp", "tp"),
        P(None, "tp", "sp"),
        P(None, "tp", "sp"),
        P(None, "tp"),
        P(None, "tp"),
        P(None, "tp"),
        P(None, "tp"),
    )
    out_specs = (P("sp", None, "tp"), P("sp", None, "tp"), P("sp", "tp", None), P(None, "tp"))
    return jax.shard_map(local, mesh=mesh, in_specs=in_specs, out_specs=out_specs, check_vma=False)
```

profile of v0, /device:TPU:0, one launch (start us, length us, event | category | flops | bytes accessed | tf_op | source)
XLA Modules:
  0.0 359.2 jit_solution(7698177402858407838)
XLA Ops:
  7.2 0.0 all-gather.6.cloned.1.call-start
  7.2 0.7 all-gather.6.cloned.1.call-update
  7.9 0.0 all-gather.8.cloned.1.call-start
  7.9 0.7 all-gather.8.cloned.1.call-update
  8.6 0.8 copy.25
  9.4 0.2 copy.26
  9.6 0.8 reshape.264
  10.4 0.1 maximum_bitcast_fusion
  10.5 0.7 reshape.296
  11.2 8.3 %all-to-all-start.2 = ((f32[16,1,160]{2,1,0:T(1,128)}), f32[16,1,160]{2,1,0:T(1,128)S(1)}, u32[]{:S(2)}, u32[]{:S(2)}) async-start(f32[16,1,160]{2,1,0:T(1,128)} %reshape.296), calls=%async_computation.2 | async-start | bytes 32768 | tf_op jit(solution)/shard_map/all_to_all | solution.py:79
  19.6 2.4 all_gather.23
  22.0 0.0 copy-start.3
  22.0 103.8 %all-gather.6.cloned.1.call-done = bf16[4096,1024]{1,0:T(8,128)(2,1)} async-done(((bf16[256,1024]{1,0:T(8,128)(2,1)}), bf16[4096,1024]{1,0:T(8,128)(2,1)}) %all-gather.6.cloned.1.call-update) | async-done | bytes 8388624 | tf_op jit(solution)/shard_map/all_gather | solution.py:84
  125.8 4.9 %convolution_convert_fusion.1 = bf16[64,1024]{1,0:T(8,128)(2,1)S(1)} fusion(bf16[4096,1024]{1,0:T(8,128)(2,1)} %all-gather.6.cloned.1.call-done, bf16[1,64,4096]{2,1,0:T(8,128)(2,1)S(1)} %all_gather.23), kind=kOutput, calls=%fused_computation.14 | convolution fusion | flops 536936448 | bytes 9043968 | tf_op jit(solution)/shard_map/dot_general | solution.py:82
  130.8 0.1 reshape_reshape.6
  130.8 1.1 pad_maximum_fusion
  131.9 0.0 all-to-all-done.2
  131.9 3.8 %all-to-all-start = ((bf16[16,20,1024]{2,1,0:T(8,128)(2,1)}), bf16[16,20,1024]{2,1,0:T(8,128)(2,1)S(1)}, u32[]{:S(2)}, u32[]{:S(2)}) async-start(bf16[16,20,1024]{2,1,0:T(8,128)(2,1)} %pad_maximum_fusion), calls=%async_computation | async-start | bytes 1572864 | tf_op jit(solution)/shard_map/all_to_all | solution.py:101
  135.7 0.0 copy-done.4
  135.7 0.6 dynamic-slice
  137.0 0.1 reduce_sum.19
  137.1 0.5 broadcast.131
  137.7 0.7 reduce.6
  138.3 0.1 reshape.297
  138.5 0.1 all_to_all.41
  138.5 0.7 all_to_all.40
  139.2 113.3 %all-gather.8.cloned.1.call-done = bf16[4096,1024]{1,0:T(8,128)(2,1)} async-done(((bf16[256,1024]{1,0:T(8,128)(2,1)}), bf16[4096,1024]{1,0:T(8,128)(2,1)}) %all-gather.8.cloned.1.call-update) | async-done | bytes 8388624 | tf_op jit(solution)/shard_map/all_gather | solution.py:89
  252.5 4.9 %convolution_convert_fusion = bf16[64,1024]{1,0:T(8,128)(2,1)S(1)} fusion(bf16[4096,1024]{1,0:T(8,128)(2,1)} %all-gather.8.cloned.1.call-done, bf16[1,64,4096]{2,1,0:T(8,128)(2,1)S(1)} %all_gather.23), kind=kOutput, calls=%fused_computation.13 | convolution fusion | flops 536936448 | bytes 9043968 | tf_op jit(solution)/shard_map/dot_general | solution.py:87
  257.5 0.1 reshape_reshape.7
  257.5 1.0 pad_maximum_fusion.1
  258.5 0.0 all-to-all-done
  258.5 3.8 %all-to-all-start.1 = ((bf16[16,20,1024]{2,1,0:T(8,128)(2,1)}), bf16[16,20,1024]{2,1,0:T(8,128)(2,1)S(1)}, u32[]{:S(2)}, u32[]{:S(2)}) async-start(bf16[16,20,1024]{2,1,0:T(8,128)(2,1)} %pad_maximum_fusion.1), calls=%async_computation.1 | async-start | bytes 1572864 | tf_op jit(solution)/shard_map/all_to_all | solution.py:102
  262.3 0.4 reshape.267
  262.7 0.3 fusion.10
  263.0 0.2 fusion.27
  263.2 0.1 fusion.22
  263.3 0.2 fusion.17
  263.5 0.1 fusion.23
  263.6 45.8 %all-reduce.2 = (f32[128]{0:T(128)S(1)}, f32[128]{0:T(128)S(1)}) all-reduce(f32[128]{0:T(128)S(1)} %fusion.22, f32[128]{0:T(128)S(1)} %fusion.23), channel_id=2, replica_groups=mesh['sp'=16,'tp'=2] {'sp'}, use_global_device_ids=true, to_apply=%add | all-reduce | flops 256 | bytes 2048
  309.4 0.1 reshape.272
  309.5 0.1 reshape.273
  309.6 0.0 all-to-all-done.1
  309.6 0.4 reshape.269
  310.0 0.4 fusion.8
  310.4 37.6 %all-gather.2 = f32[128,128]{1,0:T(8,128)S(1)} all-gather(f32[8,128]{1,0:T(8,128)S(1)} %broadcast_select_fusion), channel_id=4, replica_groups=mesh['sp'=16,'tp'=2] {'sp'}, dimensions={0}, use_global_device_ids=true | all-gather | bytes 69632 | tf_op jit(solution)/shard_map/all_gather | solution.py:14
  348.0 1.7 while.19
  348.1 0.1 fusion.36
  348.2 0.1 fusion.36
  348.3 0.1 fusion.36
  348.4 0.1 fusion.36
  348.5 0.1 fusion.36
  348.6 0.1 fusion.36
  348.7 0.1 fusion.36
  348.9 0.1 fusion.36
  349.0 0.1 fusion.36
  349.1 0.1 fusion.36
  349.2 0.1 fusion.36
  349.3 0.1 fusion.36
  349.4 0.1 fusion.36
  349.5 0.1 fusion.36
  349.6 0.1 fusion.36
  349.7 0.7 add_divide_fusion
  350.4 1.0 all_to_all.34
  351.4 1.0 all_to_all.36
  (67 shorter events, 0.6 us)
Async XLA Ops:
  7.2 118.6 %all-gather.6.cloned.1.call-start = ((), (), s32[]{:S(2)}) async-start(), calls=%async_computation.3 | async-start | bytes 8912896 | tf_op jit(solution)/shard_map/all_gather | solution.py:84
  7.9 244.6 %all-gather.8.cloned.1.call-start = ((), (), s32[]{:S(2)}) async-start(), calls=%async_computation.4 | async-start | bytes 8912896 | tf_op jit(solution)/shard_map/all_gather | solution.py:89
  11.2 120.7 %all-to-all-start.2 = ((f32[16,1,160]{2,1,0:T(1,128)}), f32[16,1,160]{2,1,0:T(1,128)S(1)}, u32[]{:S(2)}, u32[]{:S(2)}) async-start(f32[16,1,160]{2,1,0:T(1,128)} %reshape.296), calls=%async_computation.2 | async-start | bytes 32768 | tf_op jit(solution)/shard_map/all_to_all | solution.py:79
  22.0 108.9 %copy-start = (bf16[1,256,1024]{2,1,0:T(8,128)(2,1)S(1)}, bf16[1,256,1024]{2,1,0:T(8,128)(2,1)}, u32[]{:S(2)}) copy-start(bf16[1,256,1024]{2,1,0:T(8,128)(2,1)} %param.16) | copy-start | bytes 1572868
  22.0 113.8 %copy-start.4 = (bf16[1,1024]{1,0:T(2,128)(2,1)S(1)}, bf16[1,1024]{1,0:T(2,128)(2,1)}, u32[]{:S(2)}) copy-start(bf16[1,1024]{1,0:T(2,128)(2,1)} %param.22) | copy-start | bytes 6148
  22.0 113.8 %copy-start.6 = (u32[32]{0:T(128)S(1)}, u32[32]{0:T(128)}, u32[]{:S(2)}) copy-start(u32[32]{0:T(128)} %constant.87) | copy-start | bytes 388
  22.0 115.0 %copy-start.2 = (bf16[1,1024]{1,0:T(2,128)(2,1)S(1)}, bf16[1,1024]{1,0:T(2,128)(2,1)}, u32[]{:S(2)}) copy-start(bf16[1,1024]{1,0:T(2,128)(2,1)} %param.21) | copy-start | bytes 6148
  22.0 115.0 %copy-start.3 = (bf16[1,1024]{1,0:T(2,128)(2,1)S(1)}, bf16[1,1024]{1,0:T(2,128)(2,1)}, u32[]{:S(2)}) copy-start(bf16[1,1024]{1,0:T(2,128)(2,1)} %param.20) | copy-start | bytes 6148
  131.9 126.6 %all-to-all-start = ((bf16[16,20,1024]{2,1,0:T(8,128)(2,1)}), bf16[16,20,1024]{2,1,0:T(8,128)(2,1)S(1)}, u32[]{:S(2)}, u32[]{:S(2)}) async-start(bf16[16,20,1024]{2,1,0:T(8,128)(2,1)} %pad_maximum_fusion), calls=%async_computation | async-start | bytes 1572864 | tf_op jit(solution)/shard_map/all_to_all | solution.py:101
  139.2 118.3 %copy-start.1 = (bf16[1,256,1024]{2,1,0:T(8,128)(2,1)S(1)}, bf16[1,256,1024]{2,1,0:T(8,128)(2,1)}, u32[]{:S(2)}) copy-start(bf16[1,256,1024]{2,1,0:T(8,128)(2,1)} %param.17) | copy-start | bytes 1572868
  139.2 123.8 %copy-start.5 = (f32[1,8]{1,0:T(1,128)S(1)}, f32[1,8]{1,0:T(1,128)}, u32[]{:S(2)}) copy-start(f32[1,8]{1,0:T(1,128)} %param.23) | copy-start | bytes 100
  258.5 51.0 %all-to-all-start.1 = ((bf16[16,20,1024]{2,1,0:T(8,128)(2,1)}), bf16[16,20,1024]{2,1,0:T(8,128)(2,1)S(1)}, u32[]{:S(2)}, u32[]{:S(2)}) async-start(bf16[16,20,1024]{2,1,0:T(8,128)(2,1)} %pad_maximum_fusion.1), calls=%async_computation.1 | async-start | bytes 1572864 | tf_op jit(solution)/shard_map/all_to_all | solution.py:102
Sparse Core Ops, SparseCore 0:
  10.7 115.0 all-gather.5
  128.6 123.8 all-gather.7
where the time goes:
time: 360 us; the launch traced here: 359 us
  waiting for transfers between devices  218 us (61%)
  blocking collectives  85.8 us (24%)
  starting transfers between devices  16 us (4%)
  between operations  15 us (4%)
  matrix products  10.6 us (3%)
  local copies, waits for them, and re-layouts  7.49 us (2%)
  other arithmetic  5.83 us (2%)
    all_gather x1, waiting for transfers between devices, local(): lax.all_gather(value_weight, 'sp', axis=0, tiled=True)  113 us
    all_gather x1, waiting for transfers between devices, local(): lax.all_gather(key_weight, 'sp', axis=0, tiled=True)  104 us
    unnamed x1, blocking collectives  45.8 us
    all_gather x1, blocking collectives, merged_2(): gathered = jax.tree.map(lambda a: lax.all_gather(a, axis), part)  37.6 us
    all_to_all x1, starting transfers between devices, local(): lax.all_to_all(gate_block_groups, 'sp', split_axis=0, concat_axis=2, tile...  8.34 us
  transfers between devices with their start and end apart: 5, of which 2 were waited for; matrix products, arithmetic and copies ran while one was open for 5% of the time, Pallas kernels for 0%

commit v1 on v0

--- a/solution.py
+++ b/solution.py
@@ -1,6 +1,10 @@
+import functools
+
 import jax
 import jax.numpy as jnp
 from jax import lax
+from jax.experimental import pallas as pl
+from jax.experimental.pallas import tpu as pltpu
 from jax.sharding import PartitionSpec as P
 
 HEAD_DIM = 128
@@ -127,6 +131,406 @@
     return (cache_keys, stored_vector_entries, cache_gates, initial_attention_output)
 
 
+MESH = pl.DeviceIdType.MESH
+F32 = jnp.float32
+BF16 = jnp.bfloat16
+CHUNKS = 4
+
+
+def nt_dot(a, b):
+    return lax.dot_general(a, b, (((1,), (1,)), ((), ())), preferred_element_type=F32)
+
+
+def iotas(rows, columns):
+    return (
+        lax.broadcasted_iota(jnp.int32, (rows, columns), 0),
+        lax.broadcasted_iota(jnp.int32, (rows, columns), 1),
+    )
+
+
+def permuted(rows, row_source):
+    count = rows.shape[0]
+    target, source = iotas(count, count)
+    one_hot = jnp.where(source == row_source(target), 1.0, 0.0).astype(BF16)
+    return jnp.dot(one_hot, rows, preferred_element_type=F32).astype(BF16)
+
+
+def diagonal_blocks(full, heads):
+    width = full.shape[1] // heads
+    row, _ = iotas(heads, width)
+    total = jnp.zeros((heads, width), F32)
+    for head in range(heads):
+        total = jnp.where(row == head, full[:, head * width : (head + 1) * width], total)
+    return total
+
+
+def block_read(query_diagonal, keys, values, gates, gate_here, heads):
+    head_width = keys.shape[1] // heads
+    scores = nt_dot(query_diagonal, keys) * head_width ** (-0.5) + gate_here - gates
+    maximum = jnp.max(scores, axis=1, keepdims=True)
+    weights = jnp.exp(scores - maximum)
+    denominator = jnp.sum(weights, axis=1, keepdims=True)
+    upper = weights.astype(BF16)
+    lower = (weights - upper.astype(F32)).astype(BF16)
+    full = jnp.dot(upper, values, preferred_element_type=F32) + jnp.dot(
+        lower, values, preferred_element_type=F32
+    )
+    return maximum, denominator, diagonal_blocks(full, heads)
+
+
+def merge_pair(one, two):
+    maximum = jnp.maximum(one[0], two[0])
+    scale_one = jnp.exp(one[0] - maximum)
+    scale_two = jnp.exp(two[0] - maximum)
+    return (
+        maximum,
+        one[1] * scale_one + two[1] * scale_two,
+        one[2] * scale_one + two[2] * scale_two,
+    )
+
+
+def kernel(
+    n, tp, plane, dims,
+    x_ref, wk_ref, wv_ref, ek_ref, pv_ref, gg_ref, pg_ref, q_ref, sk_ref, sv_ref, sg_ref,
+    ck_ref, cv_ref, cg_ref, out_ref,
+    xp, xr, w, pf, ps, pr, pk, pv, gr, st, sr, kb, vb,
+    x_send, x_recv, w_send, w_recv, p_send, p_recv, r_send, r_recv, s_send, s_recv,
+):
+    span, past_rows, block_rows, width, heads = dims
+    depth = n // plane
+    me = lax.axis_index("sp")
+    core = lax.axis_index("tp")
+    z, p = me // plane, me % plane
+    shares = n
+    per = past_rows + block_rows
+    chunk = 2 * width // CHUNKS
+    per_matrix = width // chunk
+    features = xr.shape[2]
+
+    barrier = pltpu.get_barrier_semaphore()
+    for k in range(n):
+        for j in range(tp):
+            if k or j:
+                pl.semaphore_signal(
+                    barrier, inc=1,
+                    device_id=((me + k) % n, (core + j) % tp), device_id_type=MESH,
+                )
+    xp[...] = permuted(
+        x_ref[...],
+        lambda r: ((r % (depth * block_rows)) // block_rows * plane + r // (depth * block_rows)) * block_rows
+        + r % block_rows,
+    )
+    for c in range(CHUNKS):
+        weight = wk_ref if c < per_matrix else wv_ref
+        base = (c % per_matrix) * chunk
+        w[c, p] = weight[:, base : base + chunk]
+    pk[me] = ek_ref[me]
+    pv[me] = pv_ref[me]
+    gr[me] = gg_ref[me]
+    pl.semaphore_wait(barrier, n * tp - 1)
+
+    rows_each = depth * block_rows
+    z_each = depth // tp
+    pending = []
+    for zz in range(z_each):
+        for q in range(plane):
+            target = (core * z_each + zz) * plane + q
+            source = xp.at[q * rows_each : (q + 1) * rows_each, zz * features : (zz + 1) * features]
+            for j in range(tp):
+                index = (zz * plane + q) * tp + j
+                copy = pltpu.make_async_remote_copy(
+                    src_ref=source, dst_ref=xr.at[me],
+                    send_sem=x_send.at[index], recv_sem=x_recv.at[me],
+                    device_id=(target, (core + j) % tp), device_id_type=MESH,
+                )
+                if j:
+                    copy.start()
+                    pending.append(copy)
+                else:
+                    own = pltpu.make_async_copy(source, xr.at[me], x_recv.at[me])
+
+                    @pl.when(target != me)
+                    def _(copy=copy):
+                        copy.start()
+
+                    @pl.when(target == me)
+                    def _(own=own):
+                        own.start()
+
+    def send_weights(c):
+        weight = wk_ref if c < per_matrix else wv_ref
+        base = (c % per_matrix) * chunk
+        copies = []
+        for k in range(1, plane):
+            copy = pltpu.make_async_remote_copy(
+                src_ref=weight.at[:, base : base + chunk], dst_ref=w.at[c, p],
+                send_sem=w_send.at[c, k], recv_sem=w_recv.at[c, k],
+                device_id=(z * plane + (p + k) % plane, core), device_id_type=MESH,
+            )
+            copy.start()
+            copies.append(copy)
+        return copies
+
+    def send_past(which, source_ref, target_ref):
+        copies = []
+        for k in range(1, n):
+            target = (me + k) % n
+            copy = pltpu.make_async_remote_copy(
+                src_ref=source_ref.at[target], dst_ref=target_ref.at[me],
+                send_sem=p_send.at[which, k], recv_sem=p_recv.at[which, k],
+                device_id=(target, core), device_id_type=MESH,
+            )
+            copy.start()
+            copies.append(copy)
+        return copies
+
+    weight_copies = [send_weights(0)]
+    gate_copies = send_past(2, gg_ref, gr)
+    key_copies = send_past(0, ek_ref, pk)
+    weight_copies.append(send_weights(1))
+    value_copies = send_past(1, pv_ref, pv)
+    for c in range(2, CHUNKS):
+        weight_copies.append(send_weights(c))
+
+    row, column = iotas(heads, width)
+    query = q_ref[...].astype(F32)
+    query_diagonal = jnp.where(
+        column // (width // heads) == row, jnp.concatenate([query] * heads, axis=1), 0.0
+    ).astype(BF16)
+    gate_here = sg_ref[:, 0:1]
+    read = block_read(
+        query_diagonal,
+        ek_ref[...].reshape(n * past_rows, width),
+        pv_ref[...].reshape(n * past_rows, width),
+        pg_ref[...], gate_here, heads,
+    )
+
+    for i in range(n):
+        pltpu.make_async_copy(xr.at[i], xr.at[i], x_recv.at[i]).wait()
+    inputs = permuted(
+        xr[...].reshape(n * rows_each, features),
+        lambda r: (r % (n * block_rows)) // block_rows * rows_each
+        + r // (n * block_rows) * block_rows + r % block_rows,
+    )
+    group_rows = n * block_rows
+    partial_copies = []
+
+    def finish(c):
+        total = pf[c % 2, pl.ds(pl.multiple_of(z * group_rows, group_rows), group_rows), :]
+        for k in range(1, depth):
+            partial_copies[c][k - 1].wait_recv()
+            total = total + pr[c, k].astype(F32)
+        base = (c % per_matrix) * chunk
+        block = kb if c < per_matrix else vb
+        block[:, base : base + chunk] = total.astype(BF16)
+
+    for c in range(CHUNKS):
+        for copy in weight_copies[c]:
+            copy.wait_recv()
+        product = jnp.dot(inputs, w[c].reshape(plane * w.shape[2], chunk), preferred_element_type=F32)
+        pf[c % 2] = product
+        ps[c] = product.astype(BF16).reshape(depth, group_rows, chunk)
+        copies = []
+        for k in range(1, depth):
+            target = (z + k) % depth
+            copy = pltpu.make_async_remote_copy(
+                src_ref=ps.at[c, target], dst_ref=pr.at[c, k],
+                send_sem=r_send.at[c, k], recv_sem=r_recv.at[c, k],
+                device_id=(target * plane + p, core), device_id_type=MESH,
+            )
+            copy.start()
+            copies.append(copy)
+        partial_copies.append(copies)
+        if c:
+            finish(c - 1)
+    for copy in gate_copies:
+        copy.wait_recv()
+    _, lane = iotas(heads, gr.shape[2])
+    gates = jnp.zeros((heads, gr.shape[2]), F32)
+    for i in range(n):
+        shift = (i * block_rows - past_rows) % gr.shape[2]
+        moved = pltpu.roll(gr[i], shift, 1) if shift else gr[i]
+        gates = jnp.where(lane // block_rows == i, moved, gates)
+    finish(CHUNKS - 1)
+
+    read = merge_pair(
+        read,
+        block_read(query_diagonal, kb[...], vb[...], gates[:, :group_rows], gate_here, heads),
+    )
+    half = st.shape[1] // 2
+    _, lane = iotas(heads, st.shape[1])
+    st[0:heads, :] = jnp.where(lane < half, read[0], read[1])
+    st[heads : 2 * heads, :] = read[2]
+    stat_copies = []
+    for k in range(1, n):
+        copy = pltpu.make_async_remote_copy(
+            src_ref=st, dst_ref=sr.at[k],
+            send_sem=s_send.at[k], recv_sem=s_recv.at[k],
+            device_id=((me + k) % n, core), device_id_type=MESH,
+        )
+        copy.start()
+        stat_copies.append(copy)
+
+    def assembled(past, block):
+        rows = jnp.concatenate([past.reshape(n * past_rows, width), block], axis=0)
+
+        def row_source(r):
+            source, place = r // per, r % per
+            return jnp.where(
+                place < past_rows,
+                source * past_rows + place,
+                n * past_rows + source * block_rows + place - past_rows,
+            )
+
+        return permuted(rows, row_source)
+
+    for copy in key_copies:
+        copy.wait_recv()
+    ck_ref[...] = assembled(pk[...], kb[...])
+    for copy in value_copies:
+        copy.wait_recv()
+    cv_ref[...] = assembled(pv[...], vb[...])
+    cg_ref[...] = gr[...]
+
+    own_score = jnp.sum(query * sk_ref[...].astype(F32), axis=1, keepdims=True) * (
+        (width // heads) ** (-0.5)
+    )
+    read = merge_pair(read, (own_score, jnp.ones_like(own_score), sv_ref[...].astype(F32)))
+    for copy in stat_copies:
+        copy.wait_recv()
+    for k in range(1, n):
+        read = merge_pair(
+            read, (sr[k, 0:heads, 0:1], sr[k, 0:heads, half : half + 1], sr[k, heads : 2 * heads, :])
+        )
+    out_ref[...] = read[2] / read[1]
+
+    for zz in range(z_each):
+        for q in range(plane):
+            target = (core * z_each + zz) * plane + q
+            index = (zz * plane + q) * tp
+            source = xp.at[q * rows_each : (q + 1) * rows_each, zz * features : (zz + 1) * features]
+
+            @pl.when(target != me)
+            def _(source=source, index=index):
+                pltpu.make_async_copy(source, source, x_send.at[index]).wait()
+
+    for copy in pending:
+        copy.wait_send()
+    for copies in weight_copies + partial_copies + [gate_copies, key_copies, value_copies, stat_copies]:
+        for copy in copies:
+            copy.wait_send()
+
+
+def fused(
+    n, tp, plane,
+    block_input, key_weight, value_weight, earlier_keys, past_values, past_gates, block_gates,
+    step_query, step_key, step_value, step_gate,
+):
+    span, features_here = block_input.shape[1:]
+    kept, width = key_weight.shape
+    heads = width // HEAD_DIM
+    past_rows = earlier_keys.shape[1] // n
+    block_rows = span // n
+    depth = n // plane
+    per = past_rows + block_rows
+    lanes = HEAD_DIM
+    grouped = jnp.concatenate(
+        [
+            past_gates.reshape(heads, n, past_rows),
+            block_gates.reshape(heads, n, block_rows),
+            jnp.zeros((heads, n, lanes - per), F32),
+        ],
+        axis=2,
+    ).transpose(1, 0, 2)
+    chunk = 2 * width // CHUNKS
+    group_rows = n * block_rows
+    dims = (span, past_rows, block_rows, width, heads)
+    vmem = pl.BlockSpec(memory_space=pltpu.VMEM)
+    dma = pltpu.SemaphoreType.DMA
+    keys, values, gates, read = pl.pallas_call(
+        functools.partial(kernel, n, tp, plane, dims),
+        name="relay",
+        out_shape=(
+            jax.ShapeDtypeStruct((n * per, width), BF16),
+            jax.ShapeDtypeStruct((n * per, width), BF16),
+            jax.ShapeDtypeStruct((n, heads, lanes), F32),
+            jax.ShapeDtypeStruct((heads, HEAD_DIM), F32),
+        ),
+        in_specs=[vmem] * 11,
+        out_specs=(vmem,) * 4,
+        scratch_shapes=[
+            pltpu.VMEM((span, features_here), BF16),
+            pltpu.VMEM((n, depth * block_rows, plane * kept), BF16),
+            pltpu.VMEM((CHUNKS, plane, kept, chunk), BF16),
+            pltpu.VMEM((2, depth * group_rows, chunk), F32),
+            pltpu.VMEM((CHUNKS, depth, group_rows, chunk), BF16),
+            pltpu.VMEM((CHUNKS, depth, group_rows, chunk), BF16),
+            pltpu.VMEM((n, past_rows, width), BF16),
+            pltpu.VMEM((n, past_rows, width), BF16),
+            pltpu.VMEM((n, heads, lanes), F32),
+            pltpu.VMEM((2 * heads, HEAD_DIM), F32),
+            pltpu.VMEM((n, 2 * heads, HEAD_DIM), F32),
+            pltpu.VMEM((group_rows, width), BF16),
+            pltpu.VMEM((group_rows, width), BF16),
+            dma((depth // tp * plane * tp,)),
+            dma((n,)),
+            dma((CHUNKS, plane)),
+            dma((CHUNKS, plane)),
+            dma((3, n)),
+            dma((3, n)),
+            dma((CHUNKS, depth)),
+            dma((CHUNKS, depth)),
+            dma((n,)),
+            dma((n,)),
+        ],
+        compiler_params=pltpu.CompilerParams(
+            collective_id=0, has_side_effects=True, vmem_limit_bytes=48 * 1024 * 1024
+        ),
+    )(
+        block_input[0],
+        key_weight,
+        value_weight,
+        earlier_keys.reshape(n, past_rows, width),
+        past_values.reshape(n, past_rows, width),
+        grouped,
+        past_gates[0],
+        step_query.reshape(heads, HEAD_DIM),
+        step_key.reshape(heads, HEAD_DIM),
+        step_value.reshape(heads, HEAD_DIM),
+        jnp.broadcast_to(step_gate.reshape(heads, 1), (heads, lanes)),
+    )
+    cache_gates = gates[:, :, :per].transpose(1, 0, 2).reshape(1, heads, n * per)
+    return keys[None], values[None], cache_gates, read.reshape(1, width)
+
+
+def plane_size(n):
+    plane = 1
+    while 4 * plane * plane <= n:
+        plane *= 2
+    return plane
+
+
+def fits(n, tp, args):
+    block_input, key_weight, earlier_keys = args[0], args[1], args[3]
+    plane = plane_size(n)
+    depth = n // plane
+    span, width = block_input.shape[1], key_weight.shape[1]
+    heads = width // HEAD_DIM
+    past_rows, block_rows = earlier_keys.shape[1] // n, span // n
+    return (
+        block_input.shape[0] == 1 and n == GROUP and n % plane == 0 and depth % tp == 0
+        and span % n == 0 and past_rows % 16 == 0 and (depth * block_rows) % 16 == 0
+        and past_rows + block_rows <= HEAD_DIM and n * block_rows <= HEAD_DIM
+        and heads % 8 == 0 and width % (CHUNKS // 2 * HEAD_DIM) == 0
+    )
+
+
+def local_program(n, tp, *args):
+    if fits(n, tp, args):
+        return fused(n, tp, plane_size(n), *args)
+    return local(*args)
+
+
 def solution(mesh):
     in_specs = (
         P(None, "sp", "tp"),
@@ -142,4 +546,5 @@
         P(None, "tp"),
     )
     out_specs = (P("sp", None, "tp"), P("sp", None, "tp"), P("sp", "tp", None), P(None, "tp"))
-    return jax.shard_map(local, mesh=mesh, in_specs=in_specs, out_specs=out_specs, check_vma=False)
+    body = functools.partial(local_program, mesh.shape["sp"], mesh.shape["tp"])
+    return jax.shard_map(body, mesh=mesh, in_specs=in_specs, out_specs=out_specs, check_vma=False)

time: 360 us -> 100 us (0.28)
  waiting for transfers between devices: 218 us -> 0 us
  Pallas kernels: 0 us -> 86.5 us
  blocking collectives: 85.8 us -> 0 us
  starting transfers between devices: 16 us -> 0 us
  between operations: 15 us -> 0.72 us
  matrix products: 10.6 us -> 0 us
    all_gather x2 -> x0, waiting for transfers between devices: 217 us -> none  [the longest x1 113 us: local(): lax.all_gather(value_weight, 'sp', axis=0, tiled=True)]
    pallas_call x0 -> x1, Pallas kernels: none -> 86.5 us  [fused(): pl.pallas_call(functools.partial(kernel, n, tp, plane, dims), name='relay...]
    unnamed x1 -> x0, blocking collectives: 45.8 us -> none
    all_gather x2 -> x0, blocking collectives: 40 us -> none  [the longest x1 37.6 us: merged_2(): gathered = jax.tree.map(lambda a: lax.all_gather(a, axis), part)]
    all_to_all x3 -> x0, starting transfers between devices: 15.9 us -> none  [the longest x1 8.34 us: local(): lax.all_to_all(gate_block_groups, 'sp', split_axis=0, concat_axis=2, tile...]
    dot_general x4 -> x0, matrix products: 10.6 us -> none  [the longest x1 4.95 us: local(): jnp.dot(flat_input, lax.all_gather(value_weight, 'sp', axis=0, tiled=True...]
    unnamed x20 -> x16, local copies, waits for them, and re-layouts: 2.18 us -> 7.7 us
  transfers between devices with their start and end apart: 5 -> 0, of which waited for: 2 -> 0; matrix products, arithmetic and copies ran while one was open for 5% -> 0% of each run, Pallas kernels for 0% -> 0%
where the time goes in v1:
time: 100 us; the launch traced here: 99.7 us
  Pallas kernels  86.5 us (86%)
  local copies, waits for them, and re-layouts  10.2 us (10%)
  other arithmetic  2.26 us (2%)
    pallas_call x1, Pallas kernels, fused(): pl.pallas_call(functools.partial(kernel, n, tp, plane, dims), name='relay...  86.5 us
    unnamed x16, local copies, waits for them, and re-layouts  7.7 us
    unnamed x3, other arithmetic  2.18 us

profile of v1, /device:TPU:0, one launch (start us, length us, event | category | flops | bytes accessed | tf_op | source)
XLA Modules:
  0.0 99.7 jit_solution(14855531260402716668)
XLA Ops:
  0.6 0.0 copy-start
  0.7 0.1 pad.2.clone
  0.7 0.8 reduce
  1.5 0.7 reduce.1
  2.2 0.7 reduce.2
  2.9 0.7 broadcast_in_dim.18.sg_ref
  3.6 0.8 copy.15
  4.4 0.2 copy.17
  4.6 0.8 reshape.39
  5.4 0.0 copy-start.5
  5.4 0.1 maximum_bitcast_fusion.gg_ref
  5.5 0.0 copy-done
  5.5 0.6 copy-done.5
  6.1 0.0 copy-start.1
  6.1 1.0 %copy-done.1 = bf16[256,1024]{1,0:T(8,128)(2,1)S(1)} copy-done((bf16[256,1024]{1,0:T(8,128)(2,1)S(1)}, bf16[256,1024]{1,0:T(8,128)(2,1)}, u32[]{:S(2)}) %copy-start.1) | copy-done | bytes 524312
  7.1 0.0 copy-start.2
  7.1 1.0 %copy-done.2 = bf16[1,256,1024]{2,1,0:T(8,128)(2,1)S(1)} copy-done((bf16[1,256,1024]{2,1,0:T(8,128)(2,1)S(1)}, bf16[1,256,1024]{2,1,0:T(8,128)(2,1)}, u32[]{:S(2)}) %copy-start.2) | copy-done | bytes 524312
  8.2 0.0 copy-start.3
  8.2 1.0 %copy-done.3 = bf16[1,256,1024]{2,1,0:T(8,128)(2,1)S(1)} copy-done((bf16[1,256,1024]{2,1,0:T(8,128)(2,1)S(1)}, bf16[1,256,1024]{2,1,0:T(8,128)(2,1)}, u32[]{:S(2)}) %copy-start.3) | copy-done | bytes 524312
  9.2 0.0 copy-start.4
  9.2 0.9 copy-done.4
  10.2 86.5 %relay.1 = (bf16[320,1024]{1,0:T(8,128)(2,1)S(1)}, bf16[320,1024]{1,0:T(8,128)(2,1)S(1)}, f32[16,8,128]{2,1,0:T(8,128)S(1)}, f32[8,128]{1,0:T(8,128)S(1)}) custom-call(bf16[64,2048]{1,0:T(8,128)(2,1)S(1)} %bitcast.20, bf16[256,1024]{1,0:T(8,128)(2,1)S(1)} %copy-done, bf16[256,1024]{1,0:T(8,128)(2,1)S(1)} %copy-done.1, bf16[16,16,1024]{2,1,0:T(8,128)(2,1)S(1)} %bitcast.18, ...), custom_call_target="tpu_custom_call" | custom-call | tf_op jit(solution)/shard_map/relay/pallas_call | solution.py:450
  96.7 0.7 reshape.44
  97.4 0.8 copy.22
  98.2 0.8 copy.23
  99.1 0.6 copy.24
  (4 shorter events, 0.0 us)
Async XLA Ops:
  0.6 4.9 %copy-start = (bf16[256,1024]{1,0:T(8,128)(2,1)S(1)}, bf16[256,1024]{1,0:T(8,128)(2,1)}, u32[]{:S(2)}) copy-start(bf16[256,1024]{1,0:T(8,128)(2,1)} %wk_ref.1) | copy-start | bytes 1572868
  5.4 0.7 copy-start.5
  6.1 1.0 %copy-start.1 = (bf16[256,1024]{1,0:T(8,128)(2,1)S(1)}, bf16[256,1024]{1,0:T(8,128)(2,1)}, u32[]{:S(2)}) copy-start(bf16[256,1024]{1,0:T(8,128)(2,1)} %wv_ref.1) | copy-start | bytes 1572868
  7.1 1.0 %copy-start.2 = (bf16[1,256,1024]{2,1,0:T(8,128)(2,1)S(1)}, bf16[1,256,1024]{2,1,0:T(8,128)(2,1)}, u32[]{:S(2)}) copy-start(bf16[1,256,1024]{2,1,0:T(8,128)(2,1)} %param.14) | copy-start | bytes 1572868
  8.2 1.0 %copy-start.3 = (bf16[1,256,1024]{2,1,0:T(8,128)(2,1)S(1)}, bf16[1,256,1024]{2,1,0:T(8,128)(2,1)}, u32[]{:S(2)}) copy-start(bf16[1,256,1024]{2,1,0:T(8,128)(2,1)} %param.15) | copy-start | bytes 1572868
  9.2 0.9 copy-start.4

commit v2 on v1

--- a/solution.py
+++ b/solution.py
@@ -191,22 +191,39 @@
 
 def kernel(
     n, tp, plane, dims,
-    x_ref, wk_ref, wv_ref, ek_ref, pv_ref, gg_ref, pg_ref, q_ref, sk_ref, sv_ref, sg_ref,
+    x_hbm, wk_hbm, wv_hbm, ek_hbm, pv_hbm, pg_ref, bg_ref, q_ref, sk_ref, sv_ref, sg_ref,
     ck_ref, cv_ref, cg_ref, out_ref,
-    xp, xr, w, pf, ps, pr, pk, pv, gr, st, sr, kb, vb,
-    x_send, x_recv, w_send, w_recv, p_send, p_recv, r_send, r_recv, s_send, s_recv,
+    x_ref, ek_ref, pv_ref, gg_ref, xp, xr, w, pf, ps, pa, sb, pb, pk, pv, gr, st, sr, kb, vb,
+    l_sem, x_send, x_recv, f_send, f_recv, w_send, w_recv, p_send, p_recv, r_send, r_recv, s_send, s_recv,
 ):
     span, past_rows, block_rows, width, heads = dims
+    head_width = width // heads
     depth = n // plane
+    pairs = depth // 2
     me = lax.axis_index("sp")
     core = lax.axis_index("tp")
     z, p = me // plane, me % plane
-    shares = n
+    across, along, corner = p // 2 * 2 + 1 - p % 2, (p + 2) % plane, (p // 2 * 2 + 3 - p % 2) % plane
     per = past_rows + block_rows
     chunk = 2 * width // CHUNKS
     per_matrix = width // chunk
     features = xr.shape[2]
-
+    half_rows = w.shape[2] // 2
+    lanes = gg_ref.shape[2]
+
+    loads = [
+        pltpu.make_async_copy(x_hbm, x_ref, l_sem.at[0]),
+        pltpu.make_async_copy(ek_hbm, ek_ref, l_sem.at[1]),
+        pltpu.make_async_copy(pv_hbm, pv_ref, l_sem.at[2]),
+    ]
+    for c in range(CHUNKS):
+        weight = wk_hbm if c < per_matrix else wv_hbm
+        base = (c % per_matrix) * chunk
+        loads.append(
+            pltpu.make_async_copy(weight.at[:, base : base + chunk], w.at[c, p], l_sem.at[3 + c])
+        )
+    for load in loads:
+        load.start()
     barrier = pltpu.get_barrier_semaphore()
     for k in range(n):
         for j in range(tp):
@@ -215,15 +232,24 @@
                     barrier, inc=1,
                     device_id=((me + k) % n, (core + j) % tp), device_id_type=MESH,
                 )
+    _, lane = iotas(heads, lanes)
+    block_gates = bg_ref[...]
+    block_gates = jnp.concatenate([block_gates] * (lanes // block_gates.shape[1]), axis=1)
+    for g in range(n):
+        start = g * past_rows
+        early = pg_ref[:, start // lanes * lanes : start // lanes * lanes + lanes]
+        early = pltpu.roll(early, -start % lanes, 1) if start % lanes else early
+        shift = (past_rows - g * block_rows) % lanes
+        late = pltpu.roll(block_gates, shift, 1) if shift else block_gates
+        gg_ref[g] = jnp.where(lane < past_rows, early, late)
+    loads[0].wait()
     xp[...] = permuted(
         x_ref[...],
         lambda r: ((r % (depth * block_rows)) // block_rows * plane + r // (depth * block_rows)) * block_rows
         + r % block_rows,
     )
-    for c in range(CHUNKS):
-        weight = wk_ref if c < per_matrix else wv_ref
-        base = (c % per_matrix) * chunk
-        w[c, p] = weight[:, base : base + chunk]
+    for load in loads[1:]:
+        load.wait()
     pk[me] = ek_ref[me]
     pv[me] = pv_ref[me]
     gr[me] = gg_ref[me]
@@ -231,49 +257,60 @@
 
     rows_each = depth * block_rows
     z_each = depth // tp
-    pending = []
+
+    def input_copy(zz, q):
+        target = (core * z_each + zz) * plane + q
+        source = xp.at[q * rows_each : (q + 1) * rows_each, zz * features : (zz + 1) * features]
+        index = zz * plane + q
+        remote = pltpu.make_async_remote_copy(
+            src_ref=source, dst_ref=xr.at[me],
+            send_sem=x_send.at[index], recv_sem=x_recv.at[me],
+            device_id=(target, core), device_id_type=MESH,
+        )
+        return target, remote, pltpu.make_async_copy(source, xr.at[me], x_recv.at[me])
+
     for zz in range(z_each):
         for q in range(plane):
-            target = (core * z_each + zz) * plane + q
-            source = xp.at[q * rows_each : (q + 1) * rows_each, zz * features : (zz + 1) * features]
-            for j in range(tp):
-                index = (zz * plane + q) * tp + j
-                copy = pltpu.make_async_remote_copy(
-                    src_ref=source, dst_ref=xr.at[me],
-                    send_sem=x_send.at[index], recv_sem=x_recv.at[me],
-                    device_id=(target, (core + j) % tp), device_id_type=MESH,
-                )
-                if j:
-                    copy.start()
-                    pending.append(copy)
-                else:
-                    own = pltpu.make_async_copy(source, xr.at[me], x_recv.at[me])
-
-                    @pl.when(target != me)
-                    def _(copy=copy):
-                        copy.start()
-
-                    @pl.when(target == me)
-                    def _(own=own):
-                        own.start()
+            target, remote, own = input_copy(zz, q)
+
+            @pl.when(target != me)
+            def _(remote=remote):
+                remote.start()
+
+            @pl.when(target == me)
+            def _(own=own):
+                own.start()
+
+    def remote_weight(c, slot, source, to):
+        copy = pltpu.make_async_remote_copy(
+            src_ref=source, dst_ref=source,
+            send_sem=w_send.at[c, slot], recv_sem=w_recv.at[c, slot],
+            device_id=(z * plane + to, core), device_id_type=MESH,
+        )
+        copy.start()
+        return copy
 
     def send_weights(c):
-        weight = wk_ref if c < per_matrix else wv_ref
-        base = (c % per_matrix) * chunk
+        return [
+            remote_weight(c, 0, w.at[c, p], across),
+            remote_weight(c, 1, w.at[c, p], along),
+        ]
+
+    def forward_weights(c):
+        first, second = w.at[c, across, 0:half_rows], w.at[c, along, half_rows : 2 * half_rows]
+        weight_copies[c][0].wait_recv()
+        one = remote_weight(c, 2, first, along)
+        weight_copies[c][1].wait_recv()
+        return [one, remote_weight(c, 3, second, across)]
+
+    def await_corner(c):
+        for slot, low in ((2, 0), (3, half_rows)):
+            place = w.at[c, corner, low : low + half_rows]
+            pltpu.make_async_copy(place, place, w_recv.at[c, slot]).wait()
+
+    def send_past(which, source_ref, target_ref, offsets):
         copies = []
-        for k in range(1, plane):
-            copy = pltpu.make_async_remote_copy(
-                src_ref=weight.at[:, base : base + chunk], dst_ref=w.at[c, p],
-                send_sem=w_send.at[c, k], recv_sem=w_recv.at[c, k],
-                device_id=(z * plane + (p + k) % plane, core), device_id_type=MESH,
-            )
-            copy.start()
-            copies.append(copy)
-        return copies
-
-    def send_past(which, source_ref, target_ref):
-        copies = []
-        for k in range(1, n):
+        for k in offsets:
             target = (me + k) % n
             copy = pltpu.make_async_remote_copy(
                 src_ref=source_ref.at[target], dst_ref=target_ref.at[me],
@@ -284,20 +321,23 @@
             copies.append(copy)
         return copies
 
+    others = list(range(1, n))
+    key_copies = send_past(0, ek_ref, pk, others)
     weight_copies = [send_weights(0)]
-    gate_copies = send_past(2, gg_ref, gr)
-    key_copies = send_past(0, ek_ref, pk)
+    gate_copies = send_past(2, gg_ref, gr, others)
     weight_copies.append(send_weights(1))
-    value_copies = send_past(1, pv_ref, pv)
-    for c in range(2, CHUNKS):
-        weight_copies.append(send_weights(c))
 
     row, column = iotas(heads, width)
-    query = q_ref[...].astype(F32)
-    query_diagonal = jnp.where(
-        column // (width // heads) == row, jnp.concatenate([query] * heads, axis=1), 0.0
-    ).astype(BF16)
-    gate_here = sg_ref[:, 0:1]
+    query_wide = jnp.broadcast_to(q_ref[...].astype(F32), (heads, width))
+    query_diagonal = jnp.where(column // head_width == row, query_wide, 0.0).astype(BF16)
+    query = diagonal_blocks(query_wide, heads)
+    own_key = diagonal_blocks(jnp.broadcast_to(sk_ref[...].astype(F32), (heads, width)), heads)
+    own_value = diagonal_blocks(jnp.broadcast_to(sv_ref[...].astype(F32), (heads, width)), heads)
+    head_row, head_column = iotas(heads, heads)
+    gate_here = jnp.sum(
+        jnp.where(head_row == head_column, jnp.broadcast_to(sg_ref[...], (heads, heads)), 0.0),
+        axis=1, keepdims=True,
+    )
     read = block_read(
         query_diagonal,
         ek_ref[...].reshape(n * past_rows, width),
@@ -305,60 +345,142 @@
         pg_ref[...], gate_here, heads,
     )
 
-    for i in range(n):
-        pltpu.make_async_copy(xr.at[i], xr.at[i], x_recv.at[i]).wait()
+    holder = z // z_each
+    handed = [
+        pltpu.make_async_remote_copy(
+            src_ref=xr, dst_ref=xr, send_sem=f_send.at[j], recv_sem=f_recv.at[j],
+            device_id=(me, (core + j) % tp), device_id_type=MESH,
+        )
+        for j in range(1, tp)
+    ]
+
+    @pl.when(core == holder)
+    def _():
+        for i in range(n):
+            pltpu.make_async_copy(xr.at[i], xr.at[i], x_recv.at[i]).wait()
+        for copy in handed:
+            copy.start()
+
+    for j in range(1, tp):
+
+        @pl.when((holder + j) % tp == core)
+        def _(j=j):
+            handed[j - 1].wait_recv()
+
     inputs = permuted(
         xr[...].reshape(n * rows_each, features),
         lambda r: (r % (n * block_rows)) // block_rows * rows_each
         + r // (n * block_rows) * block_rows + r % block_rows,
     )
     group_rows = n * block_rows
-    partial_copies = []
+    forwards, first_copies, second_copies = [], [], []
+    pair, bit = z // 2, z % 2
+    mate = pair * 2 + 1 - bit
+
+    def partial_copy(c, slot, source, target_ref, to):
+        copy = pltpu.make_async_remote_copy(
+            src_ref=source, dst_ref=target_ref,
+            send_sem=r_send.at[c, slot], recv_sem=r_recv.at[c, slot],
+            device_id=(to * plane + p, core), device_id_type=MESH,
+        )
+        copy.start()
+        return copy
+
+    def own_rows(c, owner):
+        return pf[c, pl.ds(pl.multiple_of(owner * group_rows, group_rows), group_rows), :]
+
+    def multiply(c):
+        await_corner(c)
+        product = jnp.dot(inputs, w[c].reshape(plane * w.shape[2], chunk), preferred_element_type=F32)
+        pf[c] = product
+        ps[c] = product.astype(BF16).reshape(depth, group_rows, chunk)
+        copies = []
+        for o in list(range(1, pairs)) + [0]:
+            owner = (pair + o) % pairs * 2 + 1 - bit
+            copies.append(partial_copy(c, o, ps.at[c, owner], pa.at[c, o], mate))
+        first_copies.append(copies)
+
+    def pass_on(c):
+        copies = []
+        for index, o in enumerate(range(1, pairs)):
+            owner = (pair + o) % pairs * 2 + bit
+            first_copies[c][index].wait_recv()
+            sb[c, o] = (own_rows(c, owner) + pa[c, o].astype(F32)).astype(BF16)
+            copies.append(partial_copy(c, pairs + o, sb.at[c, o], pb.at[c, o], owner))
+        second_copies.append(copies)
 
     def finish(c):
-        total = pf[c % 2, pl.ds(pl.multiple_of(z * group_rows, group_rows), group_rows), :]
-        for k in range(1, depth):
-            partial_copies[c][k - 1].wait_recv()
-            total = total + pr[c, k].astype(F32)
+        first_copies[c][pairs - 1].wait_recv()
+        total = own_rows(c, z) + pa[c, 0].astype(F32)
+        for o in range(1, pairs):
+            second_copies[c][o - 1].wait_recv()
+            total = total + pb[c, o].astype(F32)
         base = (c % per_matrix) * chunk
         block = kb if c < per_matrix else vb
         block[:, base : base + chunk] = total.astype(BF16)
 
+    value_copies = []
+    cuts = [len(others) * c // 2 for c in range(3)]
     for c in range(CHUNKS):
-        for copy in weight_copies[c]:
-            copy.wait_recv()
-        product = jnp.dot(inputs, w[c].reshape(plane * w.shape[2], chunk), preferred_element_type=F32)
-        pf[c % 2] = product
-        ps[c] = product.astype(BF16).reshape(depth, group_rows, chunk)
-        copies = []
-        for k in range(1, depth):
-            target = (z + k) % depth
-            copy = pltpu.make_async_remote_copy(
-                src_ref=ps.at[c, target], dst_ref=pr.at[c, k],
-                send_sem=r_send.at[c, k], recv_sem=r_recv.at[c, k],
-                device_id=(target * plane + p, core), device_id_type=MESH,
-            )
-            copy.start()
-            copies.append(copy)
-        partial_copies.append(copies)
-        if c:
-            finish(c - 1)
+        forwards.append(forward_weights(c))
+        if c < 2:
+            value_copies += send_past(1, pv_ref, pv, others[cuts[c] : cuts[c + 1]])
+        if c + 2 < CHUNKS:
+            weight_copies.append(send_weights(c + 2))
+        if c >= 1:
+            multiply(c - 1)
+        if c >= 2:
+            pass_on(c - 2)
+        if c >= 3:
+            finish(c - 3)
+    multiply(CHUNKS - 1)
+    pass_on(CHUNKS - 2)
+    finish(CHUNKS - 3)
+
     for copy in gate_copies:
         copy.wait_recv()
-    _, lane = iotas(heads, gr.shape[2])
-    gates = jnp.zeros((heads, gr.shape[2]), F32)
+    gates = jnp.zeros((heads, lanes), F32)
+    blocks = [jnp.zeros((heads, lanes), F32) for _ in range(pl.cdiv(n * per, lanes))]
     for i in range(n):
-        shift = (i * block_rows - past_rows) % gr.shape[2]
+        shift = (i * block_rows - past_rows) % lanes
         moved = pltpu.roll(gr[i], shift, 1) if shift else gr[i]
         gates = jnp.where(lane // block_rows == i, moved, gates)
+        shift = i * per % lanes
+        moved = pltpu.roll(gr[i], shift, 1) if shift else gr[i]
+        for number in range(len(blocks)):
+            blocks[number] = jnp.where((lane + number * lanes) // per == i, moved, blocks[number])
+    for number, values in enumerate(blocks):
+        low, high = number * lanes, min((number + 1) * lanes, n * per)
+        cg_ref[:, low:high] = values[:, : high - low]
+
+    pass_on(CHUNKS - 1)
+    finish(CHUNKS - 2)
+
+    def assembled(past, block):
+        rows = jnp.concatenate([past.reshape(n * past_rows, width), block], axis=0)
+
+        def row_source(r):
+            source, place = r // per, r % per
+            return jnp.where(
+                place < past_rows,
+                source * past_rows + place,
+                n * past_rows + source * block_rows + place - past_rows,
+            )
+
+        return permuted(rows, row_source)
+
+    for copy in key_copies:
+        copy.wait_recv()
+    ck_ref[...] = assembled(pk[...], kb[...])
+    own_score = jnp.sum(query * own_key, axis=1, keepdims=True) * head_width ** (-0.5)
     finish(CHUNKS - 1)
 
     read = merge_pair(
         read,
         block_read(query_diagonal, kb[...], vb[...], gates[:, :group_rows], gate_here, heads),
     )
-    half = st.shape[1] // 2
-    _, lane = iotas(heads, st.shape[1])
+    half = head_width // 2
+    _, lane = iotas(heads, head_width)
     st[0:heads, :] = jnp.where(lane < half, read[0], read[1])
     st[heads : 2 * heads, :] = read[2]
     stat_copies = []
@@ -371,52 +493,38 @@
         copy.start()
         stat_copies.append(copy)
 
-    def assembled(past, block):
-        rows = jnp.concatenate([past.reshape(n * past_rows, width), block], axis=0)
-
-        def row_source(r):
-            source, place = r // per, r % per
-            return jnp.where(
-                place < past_rows,
-                source * past_rows + place,
-                n * past_rows + source * block_rows + place - past_rows,
-            )
-
-        return permuted(rows, row_source)
-
-    for copy in key_copies:
-        copy.wait_recv()
-    ck_ref[...] = assembled(pk[...], kb[...])
     for copy in value_copies:
         copy.wait_recv()
     cv_ref[...] = assembled(pv[...], vb[...])
-    cg_ref[...] = gr[...]
-
-    own_score = jnp.sum(query * sk_ref[...].astype(F32), axis=1, keepdims=True) * (
-        (width // heads) ** (-0.5)
-    )
-    read = merge_pair(read, (own_score, jnp.ones_like(own_score), sv_ref[...].astype(F32)))
+
+    read = merge_pair(read, (own_score, jnp.ones_like(own_score), own_value))
     for copy in stat_copies:
         copy.wait_recv()
     for k in range(1, n):
         read = merge_pair(
             read, (sr[k, 0:heads, 0:1], sr[k, 0:heads, half : half + 1], sr[k, heads : 2 * heads, :])
         )
-    out_ref[...] = read[2] / read[1]
+    result = read[2] / read[1]
+    for head in range(heads):
+        out_ref[:, head * head_width : (head + 1) * head_width] = result[head : head + 1, :]
 
     for zz in range(z_each):
         for q in range(plane):
-            target = (core * z_each + zz) * plane + q
-            index = (zz * plane + q) * tp
-            source = xp.at[q * rows_each : (q + 1) * rows_each, zz * features : (zz + 1) * features]
+            target, remote, _ = input_copy(zz, q)
 
             @pl.when(target != me)
-            def _(source=source, index=index):
-                pltpu.make_async_copy(source, source, x_send.at[index]).wait()
-
-    for copy in pending:
-        copy.wait_send()
-    for copies in weight_copies + partial_copies + [gate_copies, key_copies, value_copies, stat_copies]:
+            def _(remote=remote):
+                remote.wait_send()
+
+    @pl.when(core == holder)
+    def _():
+        for copy in handed:
+            copy.wait_send()
+
+    for copies in (
+        weight_copies + forwards + first_copies + second_copies
+        + [gate_copies, key_copies, value_copies, stat_copies]
+    ):
         for copy in copies:
             copy.wait_send()
 
@@ -434,48 +542,52 @@
     depth = n // plane
     per = past_rows + block_rows
     lanes = HEAD_DIM
-    grouped = jnp.concatenate(
-        [
-            past_gates.reshape(heads, n, past_rows),
-            block_gates.reshape(heads, n, block_rows),
-            jnp.zeros((heads, n, lanes - per), F32),
-        ],
-        axis=2,
-    ).transpose(1, 0, 2)
     chunk = 2 * width // CHUNKS
     group_rows = n * block_rows
     dims = (span, past_rows, block_rows, width, heads)
     vmem = pl.BlockSpec(memory_space=pltpu.VMEM)
+    hbm = pl.BlockSpec(memory_space=pltpu.HBM)
     dma = pltpu.SemaphoreType.DMA
+    rows = pltpu.VMEM((n, past_rows, width), BF16)
+    partials = pltpu.VMEM((CHUNKS, depth // 2, group_rows, chunk), BF16)
     keys, values, gates, read = pl.pallas_call(
         functools.partial(kernel, n, tp, plane, dims),
         name="relay",
         out_shape=(
             jax.ShapeDtypeStruct((n * per, width), BF16),
             jax.ShapeDtypeStruct((n * per, width), BF16),
-            jax.ShapeDtypeStruct((n, heads, lanes), F32),
-            jax.ShapeDtypeStruct((heads, HEAD_DIM), F32),
+            jax.ShapeDtypeStruct((heads, n * per), F32),
+            jax.ShapeDtypeStruct((1, width), F32),
         ),
-        in_specs=[vmem] * 11,
+        in_specs=[hbm] * 5 + [vmem] * 6,
         out_specs=(vmem,) * 4,
         scratch_shapes=[
             pltpu.VMEM((span, features_here), BF16),
+            rows,
+            rows,
+            pltpu.VMEM((n, heads, lanes), F32),
+            pltpu.VMEM((span, features_here), BF16),
             pltpu.VMEM((n, depth * block_rows, plane * kept), BF16),
             pltpu.VMEM((CHUNKS, plane, kept, chunk), BF16),
-            pltpu.VMEM((2, depth * group_rows, chunk), F32),
+            pltpu.VMEM((CHUNKS, depth * group_rows, chunk), F32),
             pltpu.VMEM((CHUNKS, depth, group_rows, chunk), BF16),
-            pltpu.VMEM((CHUNKS, depth, group_rows, chunk), BF16),
-            pltpu.VMEM((n, past_rows, width), BF16),
-            pltpu.VMEM((n, past_rows, width), BF16),
+            partials,
+            partials,
+            partials,
+            rows,
+            rows,
             pltpu.VMEM((n, heads, lanes), F32),
             pltpu.VMEM((2 * heads, HEAD_DIM), F32),
             pltpu.VMEM((n, 2 * heads, HEAD_DIM), F32),
             pltpu.VMEM((group_rows, width), BF16),
             pltpu.VMEM((group_rows, width), BF16),
-            dma((depth // tp * plane * tp,)),
+            dma((3 + CHUNKS,)),
+            dma((depth // tp * plane,)),
             dma((n,)),
-            dma((CHUNKS, plane)),
-            dma((CHUNKS, plane)),
+            dma((tp,)),
+            dma((tp,)),
+            dma((CHUNKS, 4)),
+            dma((CHUNKS, 4)),
             dma((3, n)),
             dma((3, n)),
             dma((CHUNKS, depth)),
@@ -492,15 +604,14 @@
         value_weight,
         earlier_keys.reshape(n, past_rows, width),
         past_values.reshape(n, past_rows, width),
-        grouped,
         past_gates[0],
-        step_query.reshape(heads, HEAD_DIM),
-        step_key.reshape(heads, HEAD_DIM),
-        step_value.reshape(heads, HEAD_DIM),
-        jnp.broadcast_to(step_gate.reshape(heads, 1), (heads, lanes)),
-    )
-    cache_gates = gates[:, :, :per].transpose(1, 0, 2).reshape(1, heads, n * per)
-    return keys[None], values[None], cache_gates, read.reshape(1, width)
+        block_gates[0],
+        step_query,
+        step_key,
+        step_value,
+        step_gate,
+    )
+    return keys[None], values[None], gates[None], read
 
 
 def plane_size(n):
@@ -518,9 +629,10 @@
     heads = width // HEAD_DIM
     past_rows, block_rows = earlier_keys.shape[1] // n, span // n
     return (
-        block_input.shape[0] == 1 and n == GROUP and n % plane == 0 and depth % tp == 0
+        block_input.shape[0] == 1 and n == GROUP and plane == 4 and n % plane == 0 and depth % (2 * tp) == 0
         and span % n == 0 and past_rows % 16 == 0 and (depth * block_rows) % 16 == 0
-        and past_rows + block_rows <= HEAD_DIM and n * block_rows <= HEAD_DIM
+        and HEAD_DIM % past_rows == 0 and past_rows + block_rows <= HEAD_DIM
+        and HEAD_DIM % span == 0
         and heads % 8 == 0 and width % (CHUNKS // 2 * HEAD_DIM) == 0
     )
 

time: 100 us -> 88.4 us (0.88)
  Pallas kernels: 86.5 us -> 75.8 us
  other arithmetic: 2.26 us -> 0 us
  local copies, waits for them, and re-layouts: 10.2 us -> 11.4 us
    pallas_call x1, Pallas kernels: 86.5 us -> 75.8 us  [fused(): pl.pallas_call(functools.partial(kernel, n, tp, plane, dims), name='relay...]
    unnamed x16 -> x26, local copies, waits for them, and re-layouts: 7.7 us -> 11.4 us
    unnamed x3 -> x0, other arithmetic: 2.18 us -> none
    reshape x4 -> x0, local copies, waits for them, and re-layouts: 1.65 us -> none  [the longest x2 0.8 us: fused(): past_gates.reshape(heads, n, past_rows)]
where the time goes in v2:
time: 88.4 us; the launch traced here: 87.9 us
  Pallas kernels  75.8 us (86%)
  local copies, waits for them, and re-layouts  11.4 us (13%)
    pallas_call x1, Pallas kernels, fused(): pl.pallas_call(functools.partial(kernel, n, tp, plane, dims), name='relay...  75.8 us
    unnamed x26, local copies, waits for them, and re-layouts  11.4 us

profile of v2, /device:TPU:0, one launch (start us, length us, event | category | flops | bytes accessed | tf_op | source)
XLA Modules:
  0.0 87.9 jit_solution(14096638152449439075)
XLA Ops:
  0.6 0.0 copy-start.5
  0.6 0.0 copy-start.10
  0.7 0.7 copy-done.5
  1.3 0.0 copy-done.10
  1.3 0.0 copy-start
  1.3 1.0 %copy-done = bf16[256,1024]{1,0:T(8,128)(2,1)S(1)} copy-done((bf16[256,1024]{1,0:T(8,128)(2,1)S(1)}, bf16[256,1024]{1,0:T(8,128)(2,1)}, u32[]{:S(2)}) %copy-start) | copy-done | bytes 524312
  2.4 0.0 copy-start.1
  2.4 1.0 %copy-done.1 = bf16[256,1024]{1,0:T(8,128)(2,1)S(1)} copy-done((bf16[256,1024]{1,0:T(8,128)(2,1)S(1)}, bf16[256,1024]{1,0:T(8,128)(2,1)}, u32[]{:S(2)}) %copy-start.1) | copy-done | bytes 524312
  3.4 0.0 copy-start.2
  3.4 1.0 %copy-done.2 = bf16[1,256,1024]{2,1,0:T(8,128)(2,1)S(1)} copy-done((bf16[1,256,1024]{2,1,0:T(8,128)(2,1)S(1)}, bf16[1,256,1024]{2,1,0:T(8,128)(2,1)}, u32[]{:S(2)}) %copy-start.2) | copy-done | bytes 524312
  4.5 0.0 copy-start.3
  4.5 1.0 %copy-done.3 = bf16[1,256,1024]{2,1,0:T(8,128)(2,1)S(1)} copy-done((bf16[1,256,1024]{2,1,0:T(8,128)(2,1)S(1)}, bf16[1,256,1024]{2,1,0:T(8,128)(2,1)}, u32[]{:S(2)}) %copy-start.3) | copy-done | bytes 524312
  5.5 0.0 copy-start.4
  5.5 0.9 %copy-done.4 = bf16[1,64,2048]{2,1,0:T(8,128)(2,1)S(1)} copy-done((bf16[1,64,2048]{2,1,0:T(8,128)(2,1)S(1)}, bf16[1,64,2048]{2,1,0:T(8,128)(2,1)}, u32[]{:S(2)}) %copy-start.4) | copy-done | bytes 262168
  6.5 0.0 copy-start.6
  6.5 0.7 copy-done.6
  7.1 0.0 copy-start.7
  7.1 0.7 copy-done.7
  7.8 0.0 copy-start.8
  7.8 0.7 copy-done.8
  8.5 0.0 copy-start.9
  8.5 0.7 copy-done.9
  9.2 75.8 %relay.1 = (bf16[320,1024]{1,0:T(8,128)(2,1)S(1)}, bf16[320,1024]{1,0:T(8,128)(2,1)S(1)}, f32[8,320]{1,0:T(8,128)S(1)}, f32[1,1024]{1,0:T(1,128)S(1)}) custom-call(bf16[64,2048]{1,0:T(8,128)(2,1)S(1)} %bitcast.12, bf16[256,1024]{1,0:T(8,128)(2,1)S(1)} %copy-done, bf16[256,1024]{1,0:T(8,128)(2,1)S(1)} %copy-done.1, bf16[16,16,1024]{2,1,0:T(8,128)(2,1)S(1)} %bitcast.10, ...), custom_call_target="tpu_custom_call" | custom-call | tf_op jit(solution)/shard_map/relay/pallas_call | solution.py:553
  85.0 0.8 copy.19
  85.9 0.8 copy.20
  86.7 0.6 copy.21
  87.3 0.6 copy.22
Async XLA Ops:
  0.6 0.7 copy-start.5
  0.6 0.7 copy-start.10
  1.3 1.0 %copy-start = (bf16[256,1024]{1,0:T(8,128)(2,1)S(1)}, bf16[256,1024]{1,0:T(8,128)(2,1)}, u32[]{:S(2)}) copy-start(bf16[256,1024]{1,0:T(8,128)(2,1)} %wk_hbm.1) | copy-start | bytes 1572868
  2.4 1.0 %copy-start.1 = (bf16[256,1024]{1,0:T(8,128)(2,1)S(1)}, bf16[256,1024]{1,0:T(8,128)(2,1)}, u32[]{:S(2)}) copy-start(bf16[256,1024]{1,0:T(8,128)(2,1)} %wv_hbm.1) | copy-start | bytes 1572868
  3.4 1.0 %copy-start.2 = (bf16[1,256,1024]{2,1,0:T(8,128)(2,1)S(1)}, bf16[1,256,1024]{2,1,0:T(8,128)(2,1)}, u32[]{:S(2)}) copy-start(bf16[1,256,1024]{2,1,0:T(8,128)(2,1)} %param.14) | copy-start | bytes 1572868
  4.5 1.0 %copy-start.3 = (bf16[1,256,1024]{2,1,0:T(8,128)(2,1)S(1)}, bf16[1,256,1024]{2,1,0:T(8,128)(2,1)}, u32[]{:S(2)}) copy-start(bf16[1,256,1024]{2,1,0:T(8,128)(2,1)} %param.15) | copy-start | bytes 1572868
  5.5 0.9 %copy-start.4 = (bf16[1,64,2048]{2,1,0:T(8,128)(2,1)S(1)}, bf16[1,64,2048]{2,1,0:T(8,128)(2,1)}, u32[]{:S(2)}) copy-start(bf16[1,64,2048]{2,1,0:T(8,128)(2,1)} %param.11) | copy-start | bytes 786436
  6.5 0.7 copy-start.6
  7.1 0.7 copy-start.7
  7.8 0.7 copy-start.8
  8.5 0.7 copy-start.9

commit v3 on v2

--- a/solution.py
+++ b/solution.py
@@ -193,8 +193,9 @@
     n, tp, plane, dims,
     x_hbm, wk_hbm, wv_hbm, ek_hbm, pv_hbm, pg_ref, bg_ref, q_ref, sk_ref, sv_ref, sg_ref,
     ck_ref, cv_ref, cg_ref, out_ref,
-    x_ref, ek_ref, pv_ref, gg_ref, xp, xr, w, pf, ps, pa, sb, pb, pk, pv, gr, st, sr, kb, vb,
-    l_sem, x_send, x_recv, f_send, f_recv, w_send, w_recv, p_send, p_recv, r_send, r_recv, s_send, s_recv,
+    x_ref, ek_ref, pv_ref, gg_ref, xp, xr, w, pf, ps, pa_k, sb_k, pb_k, pa_v, sb_v, pb_v, tk, tv, pk, pv,
+    gr, st, sr, kb, vb,
+    l_sem, x_send, x_recv, f_send, f_recv, w_send, w_recv, p_send, p_recv, d_send, d_recv, r_send, r_recv, s_send, s_recv,
 ):
     span, past_rows, block_rows, width, heads = dims
     head_width = width // heads
@@ -250,8 +251,8 @@
     )
     for load in loads[1:]:
         load.wait()
-    pk[me] = ek_ref[me]
-    pv[me] = pv_ref[me]
+    tk[z] = ek_ref[z]
+    tv[z] = pv_ref[z]
     gr[me] = gg_ref[me]
     pl.semaphore_wait(barrier, n * tp - 1)
 
@@ -308,24 +309,47 @@
             place = w.at[c, corner, low : low + half_rows]
             pltpu.make_async_copy(place, place, w_recv.at[c, slot]).wait()
 
-    def send_past(which, source_ref, target_ref, offsets):
-        copies = []
-        for k in offsets:
-            target = (me + k) % n
-            copy = pltpu.make_async_remote_copy(
-                src_ref=source_ref.at[target], dst_ref=target_ref.at[me],
-                send_sem=p_send.at[which, k], recv_sem=p_recv.at[which, k],
-                device_id=(target, core), device_id_type=MESH,
+    def start_copy(source, target_ref, sends, receives, to):
+        copy = pltpu.make_async_remote_copy(
+            src_ref=source, dst_ref=target_ref, send_sem=sends, recv_sem=receives,
+            device_id=(to, core), device_id_type=MESH,
+        )
+        copy.start()
+        return copy
+
+    def send_bundles(which, source_ref, target_ref):
+        return [
+            start_copy(
+                source_ref.at[(z + k) % depth], target_ref.at[z],
+                p_send.at[which, k], p_recv.at[which, k], (z + k) % depth * plane + p,
             )
-            copy.start()
-            copies.append(copy)
+            for k in range(1, depth)
+        ]
+
+    def distribute(which, bundles, source_ref, target_ref):
+        for copy in bundles:
+            copy.wait_recv()
+        copies = [
+            start_copy(
+                source_ref.at[:, (p + k) % plane], target_ref.at[:, p],
+                d_send.at[which, k], d_recv.at[which, k], z * plane + (p + k) % plane,
+            )
+            for k in range(1, plane)
+        ]
+        for floor in range(depth):
+            target_ref[floor, p] = source_ref[floor, p]
         return copies
 
-    others = list(range(1, n))
-    key_copies = send_past(0, ek_ref, pk, others)
-    weight_copies = [send_weights(0)]
-    gate_copies = send_past(2, gg_ref, gr, others)
-    weight_copies.append(send_weights(1))
+    gate_copies = [
+        start_copy(
+            gg_ref.at[(me + k) % n], gr.at[me],
+            d_send.at[2, k], d_recv.at[2, k], (me + k) % n,
+        )
+        for k in range(1, n)
+    ]
+    key_bundles = send_bundles(0, ek_ref, tk)
+    weight_copies = [send_weights(0), send_weights(1)]
+    value_bundles = send_bundles(1, pv_ref, tv)
 
     row, column = iotas(heads, width)
     query_wide = jnp.broadcast_to(q_ref[...].astype(F32), (heads, width))
@@ -387,30 +411,39 @@
         return copy
 
     def own_rows(c, owner):
-        return pf[c, pl.ds(pl.multiple_of(owner * group_rows, group_rows), group_rows), :]
+        return pf[c, owner]
+
+    def received(c):
+        return (pa_k, sb_k, pb_k) if c < per_matrix else (pa_v, sb_v, pb_v)
 
     def multiply(c):
         await_corner(c)
         product = jnp.dot(inputs, w[c].reshape(plane * w.shape[2], chunk), preferred_element_type=F32)
-        pf[c] = product
-        ps[c] = product.astype(BF16).reshape(depth, group_rows, chunk)
+        pf[c] = product.reshape(depth, group_rows, chunk)
+        sums = pf
+        if c >= per_matrix:
+            ps[c] = product.astype(BF16).reshape(depth, group_rows, chunk)
+            sums = ps
+        pa = received(c)[0]
         copies = []
         for o in list(range(1, pairs)) + [0]:
             owner = (pair + o) % pairs * 2 + 1 - bit
-            copies.append(partial_copy(c, o, ps.at[c, owner], pa.at[c, o], mate))
+            copies.append(partial_copy(c, o, sums.at[c, owner], pa.at[c, o], mate))
         first_copies.append(copies)
 
     def pass_on(c):
         copies = []
+        pa, sb, pb = received(c)
         for index, o in enumerate(range(1, pairs)):
             owner = (pair + o) % pairs * 2 + bit
             first_copies[c][index].wait_recv()
-            sb[c, o] = (own_rows(c, owner) + pa[c, o].astype(F32)).astype(BF16)
+            sb[c, o] = (own_rows(c, owner) + pa[c, o].astype(F32)).astype(sb.dtype)
             copies.append(partial_copy(c, pairs + o, sb.at[c, o], pb.at[c, o], owner))
         second_copies.append(copies)
 
     def finish(c):
         first_copies[c][pairs - 1].wait_recv()
+        pa, _, pb = received(c)
         total = own_rows(c, z) + pa[c, 0].astype(F32)
         for o in range(1, pairs):
             second_copies[c][o - 1].wait_recv()
@@ -419,14 +452,13 @@
         block = kb if c < per_matrix else vb
         block[:, base : base + chunk] = total.astype(BF16)
 
-    value_copies = []
-    cuts = [len(others) * c // 2 for c in range(3)]
     for c in range(CHUNKS):
         forwards.append(forward_weights(c))
-        if c < 2:
-            value_copies += send_past(1, pv_ref, pv, others[cuts[c] : cuts[c + 1]])
         if c + 2 < CHUNKS:
             weight_copies.append(send_weights(c + 2))
+        if c == CHUNKS - 1:
+            key_copies = distribute(0, key_bundles, tk, pk)
+            value_copies = distribute(1, value_bundles, tv, pv)
         if c >= 1:
             multiply(c - 1)
         if c >= 2:
@@ -523,7 +555,7 @@
 
     for copies in (
         weight_copies + forwards + first_copies + second_copies
-        + [gate_copies, key_copies, value_copies, stat_copies]
+        + [gate_copies, key_bundles, value_bundles, key_copies, value_copies, stat_copies]
     ):
         for copy in copies:
             copy.wait_send()
@@ -548,7 +580,8 @@
     vmem = pl.BlockSpec(memory_space=pltpu.VMEM)
     hbm = pl.BlockSpec(memory_space=pltpu.HBM)
     dma = pltpu.SemaphoreType.DMA
-    rows = pltpu.VMEM((n, past_rows, width), BF16)
+    rows = pltpu.VMEM((depth, plane, past_rows, width), BF16)
+    wide = pltpu.VMEM((CHUNKS, depth // 2, group_rows, chunk), F32)
     partials = pltpu.VMEM((CHUNKS, depth // 2, group_rows, chunk), BF16)
     keys, values, gates, read = pl.pallas_call(
         functools.partial(kernel, n, tp, plane, dims),
@@ -569,11 +602,16 @@
             pltpu.VMEM((span, features_here), BF16),
             pltpu.VMEM((n, depth * block_rows, plane * kept), BF16),
             pltpu.VMEM((CHUNKS, plane, kept, chunk), BF16),
-            pltpu.VMEM((CHUNKS, depth * group_rows, chunk), F32),
+            pltpu.VMEM((CHUNKS, depth, group_rows, chunk), F32),
             pltpu.VMEM((CHUNKS, depth, group_rows, chunk), BF16),
+            wide,
+            wide,
+            wide,
             partials,
             partials,
             partials,
+            rows,
+            rows,
             rows,
             rows,
             pltpu.VMEM((n, heads, lanes), F32),
@@ -588,6 +626,8 @@
             dma((tp,)),
             dma((CHUNKS, 4)),
             dma((CHUNKS, 4)),
+            dma((2, depth)),
+            dma((2, depth)),
             dma((3, n)),
             dma((3, n)),
             dma((CHUNKS, depth)),
@@ -602,8 +642,8 @@
         block_input[0],
         key_weight,
         value_weight,
-        earlier_keys.reshape(n, past_rows, width),
-        past_values.reshape(n, past_rows, width),
+        earlier_keys.reshape(depth, plane, past_rows, width),
+        past_values.reshape(depth, plane, past_rows, width),
         past_gates[0],
         block_gates[0],
         step_query,

time: 88.4 us -> 85.2 us (0.964)
  Pallas kernels: 75.8 us -> 72.6 us
    pallas_call x1, Pallas kernels: 75.8 us -> 72.6 us  [fused(): pl.pallas_call(functools.partial(kernel, n, tp, plane, dims), name='relay...]
where the time goes in v3:
time: 85.2 us; the launch traced here: 84.7 us
  Pallas kernels  72.6 us (85%)
  local copies, waits for them, and re-layouts  11.4 us (13%)
    pallas_call x1, Pallas kernels, fused(): pl.pallas_call(functools.partial(kernel, n, tp, plane, dims), name='relay...  72.6 us
    unnamed x26, local copies, waits for them, and re-layouts  11.4 us

profile of v3, /device:TPU:0, one launch (start us, length us, event | category | flops | bytes accessed | tf_op | source)
XLA Modules:
  0.0 84.7 jit_solution(12631749210187443969)
XLA Ops:
  0.6 0.0 copy-start.5
  0.6 0.0 copy-start.10
  0.7 0.7 copy-done.5
  1.3 0.0 copy-done.10
  1.3 0.0 copy-start
  1.3 1.0 %copy-done = bf16[256,1024]{1,0:T(8,128)(2,1)S(1)} copy-done((bf16[256,1024]{1,0:T(8,128)(2,1)S(1)}, bf16[256,1024]{1,0:T(8,128)(2,1)}, u32[]{:S(2)}) %copy-start) | copy-done | bytes 524312
  2.4 0.0 copy-start.1
  2.4 1.0 %copy-done.1 = bf16[256,1024]{1,0:T(8,128)(2,1)S(1)} copy-done((bf16[256,1024]{1,0:T(8,128)(2,1)S(1)}, bf16[256,1024]{1,0:T(8,128)(2,1)}, u32[]{:S(2)}) %copy-start.1) | copy-done | bytes 524312
  3.4 0.0 copy-start.2
  3.4 1.0 %copy-done.2 = bf16[1,256,1024]{2,1,0:T(8,128)(2,1)S(1)} copy-done((bf16[1,256,1024]{2,1,0:T(8,128)(2,1)S(1)}, bf16[1,256,1024]{2,1,0:T(8,128)(2,1)}, u32[]{:S(2)}) %copy-start.2) | copy-done | bytes 524312
  4.5 0.0 copy-start.3
  4.5 1.0 %copy-done.3 = bf16[1,256,1024]{2,1,0:T(8,128)(2,1)S(1)} copy-done((bf16[1,256,1024]{2,1,0:T(8,128)(2,1)S(1)}, bf16[1,256,1024]{2,1,0:T(8,128)(2,1)}, u32[]{:S(2)}) %copy-start.3) | copy-done | bytes 524312
  5.5 0.0 copy-start.4
  5.5 0.9 %copy-done.4 = bf16[1,64,2048]{2,1,0:T(8,128)(2,1)S(1)} copy-done((bf16[1,64,2048]{2,1,0:T(8,128)(2,1)S(1)}, bf16[1,64,2048]{2,1,0:T(8,128)(2,1)}, u32[]{:S(2)}) %copy-start.4) | copy-done | bytes 262168
  6.5 0.0 copy-start.6
  6.5 0.7 copy-done.6
  7.1 0.0 copy-start.7
  7.1 0.7 copy-done.7
  7.8 0.0 copy-start.8
  7.8 0.7 copy-done.8
  8.5 0.0 copy-start.9
  8.5 0.7 copy-done.9
  9.2 72.6 %relay.1 = (bf16[320,1024]{1,0:T(8,128)(2,1)S(1)}, bf16[320,1024]{1,0:T(8,128)(2,1)S(1)}, f32[8,320]{1,0:T(8,128)S(1)}, f32[1,1024]{1,0:T(1,128)S(1)}) custom-call(bf16[64,2048]{1,0:T(8,128)(2,1)S(1)} %bitcast.12, bf16[256,1024]{1,0:T(8,128)(2,1)S(1)} %copy-done, bf16[256,1024]{1,0:T(8,128)(2,1)S(1)} %copy-done.1, bf16[4,4,16,1024]{3,2,1,0:T(8,128)(2,1)S(1)} %bitcast.10, ...), custom_call_target="tpu_custom_call" | custom-call | tf_op jit(solution)/shard_map/relay/pallas_call | solution.py:586
  81.8 0.8 copy.19
  82.7 0.8 copy.20
  83.5 0.6 copy.21
  84.1 0.6 copy.22
Async XLA Ops:
  0.6 0.7 copy-start.5
  0.6 0.7 copy-start.10
  1.3 1.0 %copy-start = (bf16[256,1024]{1,0:T(8,128)(2,1)S(1)}, bf16[256,1024]{1,0:T(8,128)(2,1)}, u32[]{:S(2)}) copy-start(bf16[256,1024]{1,0:T(8,128)(2,1)} %wk_hbm.1) | copy-start | bytes 1572868
  2.4 1.0 %copy-start.1 = (bf16[256,1024]{1,0:T(8,128)(2,1)S(1)}, bf16[256,1024]{1,0:T(8,128)(2,1)}, u32[]{:S(2)}) copy-start(bf16[256,1024]{1,0:T(8,128)(2,1)} %wv_hbm.1) | copy-start | bytes 1572868
  3.4 1.0 %copy-start.2 = (bf16[1,256,1024]{2,1,0:T(8,128)(2,1)S(1)}, bf16[1,256,1024]{2,1,0:T(8,128)(2,1)}, u32[]{:S(2)}) copy-start(bf16[1,256,1024]{2,1,0:T(8,128)(2,1)} %param.14) | copy-start | bytes 1572868
  4.5 1.0 %copy-start.3 = (bf16[1,256,1024]{2,1,0:T(8,128)(2,1)S(1)}, bf16[1,256,1024]{2,1,0:T(8,128)(2,1)}, u32[]{:S(2)}) copy-start(bf16[1,256,1024]{2,1,0:T(8,128)(2,1)} %param.15) | copy-start | bytes 1572868
  5.5 0.9 %copy-start.4 = (bf16[1,64,2048]{2,1,0:T(8,128)(2,1)S(1)}, bf16[1,64,2048]{2,1,0:T(8,128)(2,1)}, u32[]{:S(2)}) copy-start(bf16[1,64,2048]{2,1,0:T(8,128)(2,1)} %param.11) | copy-start | bytes 786436
  6.5 0.7 copy-start.6
  7.1 0.7 copy-start.7
  7.8 0.7 copy-start.8
  8.5 0.7 copy-start.9
